TPU v7x, 32 devices: a whole 2x2x4 slice. The times are simulated.
32 devices in a mesh: sp: 4 (over z), dp: 8 (over y, x, core).
Axes of the slice: x: 2, y: 2, z: 4, core: 2. Of those that a mesh axis runs over, the one named last changes fastest.
Arguments:
- up_pre: bfloat16 [8, 1536, 2048], P('dp', 'sp'), may hold values from -6 to 6
- mix_pre: bfloat16 [8, 1536, 2048], P('dp', 'sp'), may hold values from -6 to 6
- ln_gain: float32 [2048], replicated, may hold values from 0.1 to 1.9
- mix_weight: bfloat16 [16, 128, 128], replicated, may hold values from -0.5 to 0.5
- mix_bias: float32 [16, 128], replicated, may hold values from 0.1 to 1.9
- out_weight: bfloat16 [2048, 2048], P('sp', 'dp'), may hold values from -0.125 to 0.125
Outputs:
- mixed_out: bfloat16 [8, 1536, 2048], P('dp', 'sp')
All inputs are finite; a program needn't handle non-finite values.
Results may differ from a plain program's by a relative error of at most 0.012.
Values may be sent and summed in bfloat16 or wider, within the bound.
A program may use at most 64 MiB of HBM per device.

v0:
```python
import jax
import jax.numpy as jnp
from jax import lax
from jax.sharding import PartitionSpec as P

BLOCK = 128


norm_epsilon = 1e-05


def normalize(up_rows, mix_rows, ln_gain):
    up_act = jax.nn.gelu(up_rows.astype(jnp.float32), approximate=False).astype(jnp.bfloat16)
    activated = jax.nn.gelu(mix_rows.astype(jnp.float32), approximate=False)
    center = jnp.mean(activated, axis=-1, keepdims=True)
    spread = jnp.mean(jnp.square(activated - center), axis=-1, keepdims=True)
    normed = ((activated - center) * lax.rsqrt(spread + norm_epsilon) * ln_gain).astype(
        jnp.bfloat16
    )
    return (up_act, normed)


def mix_blocks(up_act, normed, local_weight, local_bias):
    row_count, channels = normed.shape
    local_groups = local_weight.shape[0]
    blocks = normed.reshape(row_count // BLOCK, BLOCK, local_groups, channels // local_groups)
    mixed_sum = jnp.einsum(
        "gts,nsgc->ntgc", local_weight, blocks, preferred_element_type=jnp.float32
    )
    mixed_sum = mixed_sum + jnp.transpose(local_bias)[None, :, :, None]
    return (up_act.astype(jnp.float32) * mixed_sum.reshape(row_count, channels)).astype(
        jnp.bfloat16
    )


def per_device(up_pre, mix_pre, ln_gain, mix_weight, mix_bias, out_weight):
    up_act, normed = normalize(up_pre[0], mix_pre[0], ln_gain)
    positions = lax.broadcasted_iota(jnp.int32, (BLOCK, BLOCK), 0)
    sources = lax.broadcasted_iota(jnp.int32, (BLOCK, BLOCK), 1)
    causal = positions >= sources
    masked = jnp.where(causal[None], mix_weight, jnp.zeros_like(mix_weight))
    gated = mix_blocks(up_act, normed, masked, mix_bias)
    rows_whole = lax.all_gather(out_weight, "sp", axis=0, tiled=True)
    result = jnp.dot(
        gated,
        lax.all_gather(rows_whole, "dp", axis=1, tiled=True),
        preferred_element_type=jnp.float32,
    )
    return result.astype(jnp.bfloat16)[None]


def solution(mesh):
    return jax.shard_map(
        per_device,
        mesh=mesh,
        in_specs=(P("dp", "sp", None), P("dp", "sp", None), P(), P(), P(), P("sp", "dp")),
        out_specs=P("dp", "sp", None),
        check_vma=False,
    )
```

profile of v0, /device:TPU:0, one launch (start us, length us, event | category | flops | bytes accessed | tf_op | source)
XLA Modules:
  0.0 118.3 jit_solution(18165163851771315332)
XLA Ops:
  6.5 0.0 all-gather.3.cloned.1.call-start
  6.5 0.7 all-gather.3.cloned.1.call-update
  7.3 0.0 all-gather.5.cloned.1.call-start
  7.3 32.3 %all-gather.3.cloned.1.call-done = bf16[2048,256]{1,0:T(8,128)(2,1)} async-done(((bf16[512,256]{1,0:T(8,128)(2,1)}), bf16[2048,256]{1,0:T(8,128)(2,1)}) %all-gather.3.cloned.1.call-update) | async-done | bytes 1048592 | tf_op jit(solution)/shard_map/all_gather | solution.py:43
  39.6 0.0 all-gather.5.cloned.1.call-update
  39.7 3.6 %fusion.38 = (f32[48,8,16,128]{3,1,2,0:T(8,128)S(1)}, f32[48,8,16,128]{3,1,2,0:T(8,128)}) fusion(bf16[1,384,2048]{2,1,0:T(8,128)(2,1)} %param.7), kind=kLoop, calls=%fused_computation.45 | loop fusion | flops 3145728 | bytes 7864320
  43.2 0.7 copy.22
  43.9 2.4 %copy.13 = f32[3,128,16,128]{1,3,0,2:T(8,128)} copy(f32[3,128,16,128]{3,2,1,0:T(8,128)S(1)} %bitcast.227) | data formatting | bytes 6291456 | tf_op jit(solution)/shard_map/mul | solution.py:14
  46.3 2.9 %copy.21 = f32[48,8,16,128]{3,2,1,0:T(8,128)S(1)} copy(f32[48,8,16,128]{3,1,2,0:T(8,128)} %get-tuple-element.8) | data formatting | bytes 6291456
  49.2 2.4 %copy.18 = f32[3,128,16,128]{1,3,0,2:T(8,128)} copy(f32[3,128,16,128]{3,2,1,0:T(8,128)S(1)} %bitcast.228) | data formatting | bytes 6291456 | tf_op jit(solution)/shard_map/mul | solution.py:14
  51.7 0.0 copy-start
  51.7 0.0 copy-start.1
  51.7 0.0 copy-start.2
  51.7 0.0 copy-start.3
  51.7 0.0 copy-start.4
  51.7 8.6 %fusion.177 = (f32[384]{0:T(512)S(1)}, f32[384,2048]{1,0:T(8,128)S(1)}) fusion(bf16[1,384,2048]{2,1,0:T(8,128)(2,1)} %param.7), kind=kLoop, calls=%fused_computation.196 | loop fusion | flops 51904128 | bytes 4720128 | tf_op jit(solution)/shard_map/reduce_sum | solution.py:15
  60.4 0.5 multiply_reduce_fusion
  60.9 0.0 copy-done
  60.9 0.0 copy-done.1
  60.9 0.0 copy-done.2
  60.9 0.0 copy-done.3
  60.9 0.0 copy-done.4
  60.9 8.6 %bitcast_add_fusion = f32[3,128,16,128]{1,3,0,2:T(8,128)} fusion(f32[128,16]{0,1:T(8,128)S(1)} %bitcast.230, f32[3,128,16,128]{1,3,0,2:T(8,128)S(1)} %copy-done.1, f32[3,128,16,128]{1,3,0,2:T(8,128)S(1)} %copy-done, f32[16,128]{1,0:T(8,128)S(1)} %bitcast.231, f32[3,128]{1,0:T(4,128)S(1)} %rsqrt_bitcast_fusion, f32[3,128]{1,0:T(4,128)S(1)} %get-tuple-element.9, ...), kind=kOutput, calls=%fused_computation.82 | convolution fusion | flops 253493248 | bytes 9997312 | tf_op jit(solution)/shard_map/gts,nsgc->ntgc/dot_general | solution.py:27
  69.5 2.7 %copy.19 = f32[3,128,16,128]{3,2,1,0:T(8,128)S(1)} copy(f32[3,128,16,128]{1,3,0,2:T(8,128)} %bitcast_add_fusion) | data formatting | bytes 6291456 | tf_op jit(solution)/shard_map/add | solution.py:30
  72.2 24.6 %all-gather.5.cloned.1.call-done = bf16[2048,2048]{1,0:T(8,128)(2,1)} async-done(((bf16[2048,256]{1,0:T(8,128)(2,1)}), bf16[2048,2048]{1,0:T(8,128)(2,1)}) %all-gather.5.cloned.1.call-update) | async-done | bytes 8388624 | tf_op jit(solution)/shard_map/all_gather | solution.py:46
  96.8 14.7 %fusion.80 = bf16[1,384,2048]{2,1,0:T(8,128)(2,1)} fusion(bf16[2048,2048]{1,0:T(8,128)(2,1)} %all-gather.5.cloned.1.call-done, f32[48,8,16,128]{3,2,1,0:T(8,128)S(1)} %bitcast.229, bf16[1,384,2048]{2,1,0:T(8,128)(2,1)} %param.6), kind=kOutput, calls=%fused_computation.98 | convolution fusion | flops 3276275712 | bytes 14680064 | tf_op jit(solution)/shard_map/dot_general | solution.py:44
  (3 shorter events, 0.0 us)
Async XLA Ops:
  6.5 33.1 %all-gather.3.cloned.1.call-start = ((), (), s32[]{:S(2)}) async-start(), calls=%async_computation | async-start | bytes 1310720 | tf_op jit(solution)/shard_map/all_gather | solution.py:43
  7.3 89.5 %all-gather.5.cloned.1.call-start = ((), (), s32[]{:S(2)}) async-start(), calls=%async_computation.1 | async-start | bytes 9437184 | tf_op jit(solution)/shard_map/all_gather | solution.py:46
  51.7 9.2 %copy-start = (f32[3,128,16,128]{1,3,0,2:T(8,128)S(1)}, f32[3,128,16,128]{1,3,0,2:T(8,128)}, u32[]{:S(2)}) copy-start(f32[3,128,16,128]{1,3,0,2:T(8,128)} %copy.13) | copy-start | bytes 9437188
  51.7 9.2 %copy-start.1 = (f32[3,128,16,128]{1,3,0,2:T(8,128)S(1)}, f32[3,128,16,128]{1,3,0,2:T(8,128)}, u32[]{:S(2)}) copy-start(f32[3,128,16,128]{1,3,0,2:T(8,128)} %copy.18) | copy-start | bytes 9437188
  51.7 9.2 %copy-start.2 = (bf16[16,128,128]{2,1,0:T(8,128)(2,1)S(1)}, bf16[16,128,128]{2,1,0:T(8,128)(2,1)}, u32[]{:S(2)}) copy-start(bf16[16,128,128]{2,1,0:T(8,128)(2,1)} %param.9) | copy-start | bytes 1572868
  51.7 9.2 %copy-start.3 = (f32[16,128]{1,0:T(8,128)S(1)}, f32[16,128]{1,0:T(8,128)}, u32[]{:S(2)}) copy-start(f32[16,128]{1,0:T(8,128)} %param.10) | copy-start | bytes 24580
  51.7 9.2 %copy-start.4 = (f32[2048]{0:T(1024)S(1)}, f32[2048]{0:T(1024)}, u32[]{:S(2)}) copy-start(f32[2048]{0:T(1024)} %param.8) | copy-start | bytes 24580
Sparse Core Ops, SparseCore 0:
  8.9 30.6 all-gather.2
  41.5 55.2 all-gather.4
where the time goes:
time: 118 us
  waiting for transfers between devices  57.7 us (49%)
  matrix products  23.3 us (20%)
  between operations  13.5 us (11%)
  other arithmetic  12.7 us (11%)
  local copies, waits for them, and re-layouts  11.1 us (9%)
    all_gather x1, waiting for transfers between devices, per_device(): rows_whole = lax.all_gather(out_weight, 'sp', axis=0, tiled=True)  32.3 us
    all_gather x1, waiting for transfers between devices, per_device(): lax.all_gather(rows_whole, 'dp', axis=1, tiled=True)  24.6 us
    dot_general x1, matrix products, per_device(): jnp.dot(gated, lax.all_gather(rows_whole, 'dp', axis=1, tiled=True), pref...  14.7 us
    reduce_sum x1, other arithmetic, normalize(): center = jnp.mean(activated, axis=-1, keepdims=True)  8.65 us
    dot_general x1, matrix products, mix_blocks(): jnp.einsum('gts,nsgc->ntgc', local_weight, blocks, preferred_element_type...  8.6 us
    mul x2, local copies, waits for them, and re-layouts, normalize(): activated = jax.nn.gelu(mix_rows.astype(jnp.float32), approximate=False)  4.86 us
    unnamed x1, other arithmetic  3.58 us
    unnamed x12, local copies, waits for them, and re-layouts  3.57 us
  transfers between devices with their start and end apart: 2, of which 2 were waited for; matrix products, arithmetic and copies ran while one was open for 27% of the time, Pallas kernels for 0%

commit v1 on v0

v1 whole, which is shorter than its diff:
```python
import functools

import jax
import jax.numpy as jnp
from jax import lax
from jax.experimental import pallas as pl
from jax.experimental.pallas import tpu as pltpu
from jax.sharding import PartitionSpec as P

BLOCK = 128
LANES = 128
CHUNK = 16
MESH = pl.DeviceIdType.MESH

norm_epsilon = 1e-05


def gelu(values):
    return 0.5 * values * (1.0 + lax.erf(values * 0.7071067811865476))


def slot_list(depth):
    slots = [("own", 0)]
    for hop in range(1, depth):
        slots += [("up", hop), ("down", hop)]
    return slots


def kernel(
    depth, rows_c,
    up_hbm, mix_hbm, gain_ref, weight_hbm, bias_ref, shard_hbm,
    out_ref,
    held, up_buf, mix_buf, weight_buf, masked, bias_full, normed, up_act, gated, total,
    in_sem, send_sem, recv_sem,
):
    rows, channels = up_hbm.shape
    groups = weight_hbm.shape[0]
    width = channels // groups
    block_count = rows // BLOCK
    shard_rows, shard_cols = shard_hbm.shape
    chips = held.shape[1]
    rows_ab = shard_rows - rows_c
    rows_a = rows_ab // 32 * 16

    z = lax.axis_index("sp")
    d = lax.axis_index("dp")
    core = lax.rem(d, 2)
    chip = d // 2
    x = lax.rem(chip, 2)
    y = chip // 2
    chip_x = chip + 1 - 2 * x
    chip_y = chip + 2 - 4 * y
    chip_xy = chip_x + 2 - 4 * y
    to_x = {"dp": chip_x * 2 + core}
    to_y = {"dp": chip_y * 2 + core}
    partner = {"dp": chip * 2 + 1 - core}
    above = {"sp": z + 1}
    below = {"sp": z - 1}
    has_above = z < depth - 1
    has_below = z > 0

    def held_at(cc, q, origin, part):
        start, count = {
            "a": (0, rows_a),
            "b": (rows_a, rows_ab - rows_a),
            "ab": (0, rows_ab),
            "c": (rows_ab, rows_c),
            "all": (0, shard_rows),
        }[part]
        place = pl.ds(pl.multiple_of(origin * shard_rows + start, 16), count)
        return held.at[cc, q, place, :]

    names = {}

    def index(name):
        return names.setdefault(name, len(names))

    def copy(ref, name, target):
        k = index(name)
        return pltpu.make_async_remote_copy(
            src_ref=ref, dst_ref=ref, send_sem=send_sem.at[k], recv_sem=recv_sem.at[k],
            device_id=target, device_id_type=MESH,
        )

    slots = slot_list(depth)

    def origin_of(n):
        way, hop = slots[n]
        return z if way == "own" else z - hop if way == "up" else z + hop

    def when(n, body):
        way, hop = slots[n]
        if way == "own":
            body()
        elif way == "up":
            pl.when(z >= hop)(body)
        else:
            pl.when(z <= depth - 1 - hop)(body)

    def sends(n):
        way, hop = slots[n]
        o = origin_of(n)
        if way in ("own", "up") and hop + 1 < depth:
            @pl.when(has_above)
            def _():
                copy(held_at(core, chip, o, "ab"), ("z", "up", hop + 1), above).start()
        if way in ("own", "down") and hop + 1 < depth:
            @pl.when(has_below)
            def _():
                copy(held_at(core, chip, o, "ab"), ("z", "down", hop + 1), below).start()
        copy(held_at(core, chip, o, "a"), ("xa", n), to_x).start()
        copy(held_at(core, chip, o, "b"), ("yb", n), to_y).start()
        copy(held_at(core, chip, o, "b"), ("xb", n), to_x).start()
        copy(held_at(core, chip, o, "a"), ("ya", n), to_y).start()

    def recv_z(n):
        def body():
            way, hop = slots[n]
            copy(held_at(core, chip, origin_of(n), "ab"), ("z", way, hop), above).wait_recv()
            sends(n)
        when(n, body)

    def turn(n):
        def body():
            o = origin_of(n)
            copy(held_at(core, chip_x, o, "a"), ("xa", n), to_x).wait_recv()
            copy(held_at(core, chip_x, o, "a"), ("ya2", n), to_y).start()
            copy(held_at(core, chip_y, o, "b"), ("yb", n), to_y).wait_recv()
            copy(held_at(core, chip_y, o, "b"), ("xb2", n), to_x).start()
        when(n, body)

    def finish(n):
        def body():
            o = origin_of(n)
            copy(held_at(core, chip_x, o, "b"), ("xb", n), to_x).wait_recv()
            copy(held_at(core, chip_y, o, "a"), ("ya", n), to_y).wait_recv()
            copy(held_at(core, chip_xy, o, "b"), ("xb2", n), to_x).wait_recv()
            copy(held_at(core, chip_xy, o, "a"), ("ya2", n), to_y).wait_recv()
            copy(held_at(core, slice(None), o, "ab"), ("p", n), partner).start()
        when(n, body)

    def recv_partner(n):
        def body():
            o = origin_of(n)
            copy(held_at(1 - core, slice(None), o, "ab"), ("p", n), partner).wait_recv()
            if rows_c:
                copy(held_at(1 - core, slice(None), o, "c"), ("pc", n), partner).wait_recv()
        when(n, body)

    def c_pass(n):
        way, hop = slots[n]
        o = origin_of(n)
        if way in ("own", "up") and hop + 1 < depth:
            @pl.when(has_above)
            def _():
                copy(held_at(core, slice(None), o, "c"), ("zc", "up", hop + 1), above).start()
        if way in ("own", "down") and hop + 1 < depth:
            @pl.when(has_below)
            def _():
                copy(held_at(core, slice(None), o, "c"), ("zc", "down", hop + 1), below).start()
        copy(held_at(core, slice(None), o, "c"), ("pc", n), partner).start()

    def c_start():
        if rows_c:
            copy(held_at(core, chip, z, "c"), ("cx",), to_x).start()
            copy(held_at(core, chip, z, "c"), ("cy",), to_y).start()

    def c_turn():
        if rows_c:
            copy(held_at(core, chip_x, z, "c"), ("cx",), to_x).wait_recv()
            copy(held_at(core, chip_x, z, "c"), ("cy2",), to_y).start()

    def c_layer():
        if rows_c:
            copy(held_at(core, chip_y, z, "c"), ("cy",), to_y).wait_recv()
            copy(held_at(core, chip_xy, z, "c"), ("cy2",), to_y).wait_recv()
            c_pass(0)

    def c_recv(n):
        if rows_c:
            def body():
                way, hop = slots[n]
                copy(held_at(core, slice(None), origin_of(n), "c"), ("zc", way, hop), above).wait_recv()
                c_pass(n)
            when(n, body)

    own = pltpu.make_async_copy(shard_hbm, held_at(core, chip, z, "all"), in_sem.at[0])
    own.start()
    loads = []
    for b in range(block_count):
        place = pl.ds(b * BLOCK, BLOCK)
        loads.append((
            pltpu.make_async_copy(mix_hbm.at[place], mix_buf.at[place], in_sem.at[2 + 2 * b]),
            pltpu.make_async_copy(up_hbm.at[place], up_buf.at[place], in_sem.at[3 + 2 * b]),
        ))
        loads[-1][0].start()
        loads[-1][1].start()
    weights = pltpu.make_async_copy(weight_hbm, weight_buf, in_sem.at[1])
    weights.start()

    barrier = pltpu.get_barrier_semaphore()
    for target in (to_x, to_y, partner):
        pl.semaphore_signal(barrier, inc=1, device_id=target, device_id_type=MESH)

    @pl.when(has_above)
    def _():
        pl.semaphore_signal(barrier, inc=1, device_id=above, device_id_type=MESH)

    @pl.when(has_below)
    def _():
        pl.semaphore_signal(barrier, inc=1, device_id=below, device_id_type=MESH)

    pl.semaphore_wait(barrier, 3 + has_above.astype(jnp.int32) + has_below.astype(jnp.int32))

    own.wait()
    sends(0)
    c_start()

    def prepare():
        weights.wait()
        positions = lax.broadcasted_iota(jnp.int32, (BLOCK, BLOCK), 0)
        sources = lax.broadcasted_iota(jnp.int32, (BLOCK, BLOCK), 1)

        def one(g, carry):
            kept = weight_buf[g].astype(jnp.float32)
            masked[g] = jnp.where(positions >= sources, kept, 0.0).astype(jnp.bfloat16)
            bias_full[g] = jnp.broadcast_to(bias_ref[pl.ds(g, 1), :], (BLOCK, BLOCK)).T
            return carry

        lax.fori_loop(0, groups, one, 0)

    def activate(b, first, last):
        def one(i, carry):
            place = pl.ds(pl.multiple_of(i * CHUNK, CHUNK), CHUNK)
            source = pl.ds(pl.multiple_of(b * BLOCK + i * CHUNK, CHUNK), CHUNK)
            activated = gelu(mix_buf[source, :].astype(jnp.float32))
            center = jnp.sum(activated, axis=-1, keepdims=True) * (1.0 / channels)
            activated = activated - center
            spread = jnp.sum(activated * activated, axis=-1, keepdims=True) * (1.0 / channels)
            scale = lax.rsqrt(spread + norm_epsilon)
            normed[place, :] = (activated * scale * gain_ref[...]).astype(jnp.bfloat16)
            up_act[place, :] = gelu(up_buf[source, :].astype(jnp.float32)).astype(jnp.bfloat16)
            return carry

        lax.fori_loop(first, last, one, 0)

    def mix(b):
        def one(g, carry):
            cols = pl.ds(pl.multiple_of(g * width, LANES), width)
            mixed = jnp.dot(masked[g], normed[:, cols], preferred_element_type=jnp.float32)
            spread_bias = jnp.concatenate([bias_full[g]] * (width // BLOCK), axis=1)
            gated[pl.ds(b * BLOCK, BLOCK), cols] = (
                up_act[:, cols].astype(jnp.float32) * (mixed + spread_bias)
            ).astype(jnp.bfloat16)
            return carry

        lax.fori_loop(0, groups, one, 0)

    def project(n):
        def body():
            o = origin_of(n)
            left = gated[:, pl.ds(pl.multiple_of(o * shard_rows, LANES), shard_rows)]
            depth_rows = pl.ds(pl.multiple_of(o * shard_rows, 16), shard_rows)

            def one(j, carry):
                cols = pl.ds(pl.multiple_of(j * shard_cols, LANES), shard_cols)
                term = jnp.dot(
                    left, held[lax.rem(j, 2), j // 2, depth_rows, :],
                    preferred_element_type=jnp.float32,
                )
                if n == 0:
                    total[:, cols] = term
                else:
                    total[:, cols] += term
                return carry

            lax.fori_loop(0, 2 * chips, one, 0)
        when(n, body)

    per_block = BLOCK // CHUNK
    half = per_block // 2

    events = [[lambda: turn(0)]]
    for hop in range(1, depth):
        up, down = 2 * hop - 1, 2 * hop
        group = [functools.partial(recv_z, up), functools.partial(recv_z, down)]
        events.append(group)
        if hop == 1:
            events.append([c_turn])
        events.append([functools.partial(turn, up), functools.partial(turn, down)])
        if hop == 1:
            events.append([c_layer])
        if hop > 1:
            events.append([functools.partial(c_recv, up - 2), functools.partial(c_recv, down - 2)])
    work = [prepare]
    for b in range(block_count):
        def load(b=b):
            loads[b][0].wait()
            loads[b][1].wait()
            activate(b, 0, half)
        work += [load, functools.partial(activate, b, half, per_block), functools.partial(mix, b)]
    while events or work:
        for _ in range(2 if len(work) > 8 else 1):
            if work:
                work.pop(0)()
        if events:
            for event in events.pop(0):
                event()

    last = len(slots) - 2
    finish(0)
    finish(1)
    finish(2)
    recv_partner(0)
    project(0)
    for n in range(3, len(slots)):
        finish(n)
    c_recv(last)
    c_recv(last + 1)
    for n in range(1, len(slots)):
        recv_partner(n)
        project(n)
    out_ref[...] = total[...].astype(out_ref.dtype)

    for n in range(len(slots)):
        way, hop = slots[n]

        def body():
            o = origin_of(n)
            for name, part in (("xa", "a"), ("yb", "b"), ("xb", "b"), ("ya", "a"), ("ya2", "a"), ("xb2", "b")):
                copy(held_at(core, chip, o, part), (name, n), to_x).wait_send()
            copy(held_at(core, slice(None), o, "ab"), ("p", n), partner).wait_send()
            if rows_c:
                copy(held_at(core, slice(None), o, "c"), ("pc", n), partner).wait_send()
            for direction, cond, target in (("up", has_above, above), ("down", has_below, below)):
                if way in ("own", direction) and hop + 1 < depth:
                    @pl.when(cond)
                    def _():
                        copy(held_at(core, chip, o, "ab"), ("z", direction, hop + 1), target).wait_send()
                        if rows_c:
                            copy(held_at(core, slice(None), o, "c"), ("zc", direction, hop + 1), target).wait_send()
        when(n, body)
    if rows_c:
        for name in ("cx", "cy", "cy2"):
            copy(held_at(core, chip, z, "c"), (name,), to_x).wait_send()


def semaphores(depth):
    return 10 * (2 * depth - 1) + 3


def fused(depth, columns, up_rows, mix_rows, ln_gain, mix_weight, mix_bias, out_weight):
    rows, channels = up_rows.shape
    groups = mix_weight.shape[0]
    shard_rows, shard_cols = out_weight.shape
    chips = columns // 2
    rows_c = shard_rows * 3 // 16 // 32 * 32
    any_space = pl.BlockSpec(memory_space=pl.ANY)
    vmem = pl.BlockSpec(memory_space=pltpu.VMEM)
    return pl.pallas_call(
        functools.partial(kernel, depth, rows_c),
        out_shape=jax.ShapeDtypeStruct((rows, shard_cols * columns), jnp.bfloat16),
        in_specs=[any_space, any_space, vmem, any_space, vmem, any_space],
        out_specs=vmem,
        scratch_shapes=[
            pltpu.VMEM((2, chips, depth * shard_rows, shard_cols), jnp.bfloat16),
            pltpu.VMEM((rows, channels), jnp.bfloat16),
            pltpu.VMEM((rows, channels), jnp.bfloat16),
            pltpu.VMEM((groups, BLOCK, BLOCK), jnp.bfloat16),
            pltpu.VMEM((groups, BLOCK, BLOCK), jnp.bfloat16),
            pltpu.VMEM((groups, BLOCK, BLOCK), jnp.float32),
            pltpu.VMEM((BLOCK, channels), jnp.bfloat16),
            pltpu.VMEM((BLOCK, channels), jnp.bfloat16),
            pltpu.VMEM((rows, channels), jnp.bfloat16),
            pltpu.VMEM((rows, shard_cols * columns), jnp.float32),
            pltpu.SemaphoreType.DMA((2 + 2 * (rows // BLOCK),)),
            pltpu.SemaphoreType.DMA((semaphores(depth),)),
            pltpu.SemaphoreType.DMA((semaphores(depth),)),
        ],
        compiler_params=pltpu.CompilerParams(
            collective_id=0, has_side_effects=True, vmem_limit_bytes=60 * 2**20
        ),
    )(up_rows, mix_rows, ln_gain[None], mix_weight, mix_bias, out_weight)


def plain(up_rows, mix_rows, ln_gain, mix_weight, mix_bias, out_weight):
    up_act = gelu(up_rows.astype(jnp.float32)).astype(jnp.bfloat16)
    activated = gelu(mix_rows.astype(jnp.float32))
    center = jnp.mean(activated, axis=-1, keepdims=True)
    spread = jnp.mean(jnp.square(activated - center), axis=-1, keepdims=True)
    normed = ((activated - center) * lax.rsqrt(spread + norm_epsilon) * ln_gain).astype(
        jnp.bfloat16
    )
    positions = lax.broadcasted_iota(jnp.int32, (BLOCK, BLOCK), 0)
    sources = lax.broadcasted_iota(jnp.int32, (BLOCK, BLOCK), 1)
    masked = jnp.where((positions >= sources)[None], mix_weight, jnp.zeros_like(mix_weight))
    row_count, channels = normed.shape
    groups = masked.shape[0]
    blocks = normed.reshape(row_count // BLOCK, BLOCK, groups, channels // groups)
    mixed = jnp.einsum("gts,nsgc->ntgc", masked, blocks, preferred_element_type=jnp.float32)
    mixed = mixed + jnp.transpose(mix_bias)[None, :, :, None]
    gated = (up_act.astype(jnp.float32) * mixed.reshape(row_count, channels)).astype(jnp.bfloat16)
    rows_whole = lax.all_gather(out_weight, "sp", axis=0, tiled=True)
    whole = lax.all_gather(rows_whole, "dp", axis=1, tiled=True)
    return jnp.dot(gated, whole, preferred_element_type=jnp.float32).astype(jnp.bfloat16)


def solution(mesh):
    depth, columns = mesh.shape["sp"], mesh.shape["dp"]

    def per_device(up_pre, mix_pre, ln_gain, mix_weight, mix_bias, out_weight):
        shard_rows, shard_cols = out_weight.shape
        fits = (
            columns == 8
            and depth > 1
            and up_pre.shape[0] == 1
            and shard_cols % LANES == 0
            and shard_rows % LANES == 0
            and up_pre.shape[1] % BLOCK == 0
            and up_pre.shape[2] % (mix_weight.shape[0] * LANES) == 0
        )
        form = functools.partial(fused, depth, columns) if fits else plain
        return form(up_pre[0], mix_pre[0], ln_gain, mix_weight, mix_bias, out_weight)[None]

    return jax.shard_map(
        per_device,
        mesh=mesh,
        in_specs=(P("dp", "sp", None), P("dp", "sp", None), P(), P(), P(), P("sp", "dp")),
        out_specs=P("dp", "sp", None),
        check_vma=False,
    )
```

time: 118 us -> 56.4 us (0.48)
  waiting for transfers between devices: 57.7 us -> 0 us
  Pallas kernels: 0 us -> 53.4 us
  matrix products: 23.3 us -> 0 us
  between operations: 13.5 us -> 0.01 us
  other arithmetic: 12.7 us -> 0 us
  local copies, waits for them, and re-layouts: 11.1 us -> 2.73 us
    all_gather x2 -> x0, waiting for transfers between devices: 57 us -> none  [the longest x1 32.3 us: per_device(): rows_whole = lax.all_gather(out_weight, 'sp', axis=0, tiled=True)]
    pallas_call x0 -> x1, Pallas kernels: none -> 53.4 us  [fused(): pl.pallas_call(functools.partial(kernel, depth, rows_c), out_shape=jax.Sh...]
    dot_general x2 -> x0, matrix products: 23.3 us -> none  [the longest x1 14.7 us: per_device(): jnp.dot(gated, lax.all_gather(rows_whole, 'dp', axis=1, tiled=True), pref...]
    reduce_sum x2 -> x0, other arithmetic: 9.1 us -> none  [the longest x1 8.65 us: normalize(): center = jnp.mean(activated, axis=-1, keepdims=True)]
    mul x2 -> x0, local copies, waits for them, and re-layouts: 4.86 us -> none  [normalize(): activated = jax.nn.gelu(mix_rows.astype(jnp.float32), approximate=False)]
    unnamed x1 -> x0, other arithmetic: 3.58 us -> none
    add x1 -> x0, local copies, waits for them, and re-layouts: 2.65 us -> none  [mix_blocks(): mixed_sum = mixed_sum + jnp.transpose(local_bias)[None, :, :, None]]
    unnamed x12 -> x1, local copies, waits for them, and re-layouts: 3.57 us -> 2.73 us
  transfers between devices with their start and end apart: 2 -> 0, of which waited for: 2 -> 0; matrix products, arithmetic and copies ran while one was open for 27% -> 0% of each run, Pallas kernels for 0% -> 0%
where the time goes in v1:
time: 56.4 us; the launch traced here: 56.2 us
  Pallas kernels  53.4 us (95%)
  local copies, waits for them, and re-layouts  2.73 us (5%)
    pallas_call x1, Pallas kernels, fused(): pl.pallas_call(functools.partial(kernel, depth, rows_c), out_shape=jax.Sh...  53.4 us
    unnamed x1, local copies, waits for them, and re-layouts  2.73 us

profile of v1, /device:TPU:0, one launch (start us, length us, event | category | flops | bytes accessed | tf_op | source)
XLA Modules:
  0.0 56.2 jit_solution(5437137985191671691)
XLA Ops:
  0.0 53.4 %shard_map.64 = bf16[384,2048]{1,0:T(8,128)(2,1)} custom-call(bf16[384,2048]{1,0:T(8,128)(2,1)} %bitcast.5, bf16[384,2048]{1,0:T(8,128)(2,1)} %bitcast.6, f32[1,2048]{1,0:T(1,128)} %bitcast.7, bf16[16,128,128]{2,1,0:T(8,128)(2,1)} %weight_hbm.1, f32[16,128]{1,0:T(8,128)} %bias_ref.1, bf16[512,256]{1,0:T(8,128)(2,1)} %shard_hbm.1), custom_call_target="tpu_custom_call" | custom-call | tf_op jit(solution)/shard_map/pallas_call | solution.py:360
  53.5 2.7 %copy.8 = bf16[1,384,2048]{2,1,0:T(8,128)(2,1)} copy(bf16[1,384,2048]{2,1,0:T(8,128)(2,1)} %bitcast.4) | data formatting | bytes 3145728

commit v2 on v1

--- a/solution.py
+++ b/solution.py
@@ -28,9 +28,9 @@
 
 def kernel(
     depth, rows_c,
-    up_hbm, mix_hbm, gain_ref, weight_hbm, bias_ref, shard_hbm,
+    up_hbm, mix_hbm, gain_hbm, weight_hbm, bias_hbm, shard_hbm,
     out_ref,
-    held, up_buf, mix_buf, weight_buf, masked, bias_full, normed, up_act, gated, total,
+    held, gain_ref, bias_ref, up_buf, mix_buf, weight_buf, masked, bias_full, normed, up_act, gated, total,
     in_sem, send_sem, recv_sem,
 ):
     rows, channels = up_hbm.shape
@@ -112,6 +112,7 @@
         copy(held_at(core, chip, o, "b"), ("yb", n), to_y).start()
         copy(held_at(core, chip, o, "b"), ("xb", n), to_x).start()
         copy(held_at(core, chip, o, "a"), ("ya", n), to_y).start()
+        copy(held_at(core, chip, o, "ab"), ("p", 0, n), partner).start()
 
     def recv_z(n):
         def body():
@@ -133,16 +134,19 @@
         def body():
             o = origin_of(n)
             copy(held_at(core, chip_x, o, "b"), ("xb", n), to_x).wait_recv()
+            copy(held_at(core, chip_x, o, "ab"), ("p", 1, n), partner).start()
             copy(held_at(core, chip_y, o, "a"), ("ya", n), to_y).wait_recv()
+            copy(held_at(core, chip_y, o, "ab"), ("p", 2, n), partner).start()
             copy(held_at(core, chip_xy, o, "b"), ("xb2", n), to_x).wait_recv()
             copy(held_at(core, chip_xy, o, "a"), ("ya2", n), to_y).wait_recv()
-            copy(held_at(core, slice(None), o, "ab"), ("p", n), partner).start()
+            copy(held_at(core, chip_xy, o, "ab"), ("p", 3, n), partner).start()
         when(n, body)
 
     def recv_partner(n):
         def body():
             o = origin_of(n)
-            copy(held_at(1 - core, slice(None), o, "ab"), ("p", n), partner).wait_recv()
+            for k, q in enumerate((chip, chip_x, chip_y, chip_xy)):
+                copy(held_at(1 - core, q, o, "ab"), ("p", k, n), partner).wait_recv()
             if rows_c:
                 copy(held_at(1 - core, slice(None), o, "c"), ("pc", n), partner).wait_recv()
         when(n, body)
@@ -186,6 +190,11 @@
 
     own = pltpu.make_async_copy(shard_hbm, held_at(core, chip, z, "all"), in_sem.at[0])
     own.start()
+    weights = pltpu.make_async_copy(weight_hbm, weight_buf, in_sem.at[1])
+    gain = pltpu.make_async_copy(gain_hbm, gain_ref, in_sem.at[2 + 2 * block_count])
+    bias = pltpu.make_async_copy(bias_hbm, bias_ref, in_sem.at[3 + 2 * block_count])
+    for part in (weights, gain, bias):
+        part.start()
     loads = []
     for b in range(block_count):
         place = pl.ds(b * BLOCK, BLOCK)
@@ -195,8 +204,6 @@
         ))
         loads[-1][0].start()
         loads[-1][1].start()
-    weights = pltpu.make_async_copy(weight_hbm, weight_buf, in_sem.at[1])
-    weights.start()
 
     barrier = pltpu.get_barrier_semaphore()
     for target in (to_x, to_y, partner):
@@ -213,11 +220,13 @@
     pl.semaphore_wait(barrier, 3 + has_above.astype(jnp.int32) + has_below.astype(jnp.int32))
 
     own.wait()
+    c_start()
     sends(0)
-    c_start()
 
     def prepare():
         weights.wait()
+        gain.wait()
+        bias.wait()
         positions = lax.broadcasted_iota(jnp.int32, (BLOCK, BLOCK), 0)
         sources = lax.broadcasted_iota(jnp.int32, (BLOCK, BLOCK), 1)
 
@@ -242,7 +251,7 @@
             up_act[place, :] = gelu(up_buf[source, :].astype(jnp.float32)).astype(jnp.bfloat16)
             return carry
 
-        lax.fori_loop(first, last, one, 0)
+        lax.fori_loop(first, last, one, 0, unroll=2)
 
     def mix(b):
         def one(g, carry):
@@ -254,18 +263,18 @@
             ).astype(jnp.bfloat16)
             return carry
 
-        lax.fori_loop(0, groups, one, 0)
-
-    def project(n):
+        lax.fori_loop(0, groups, one, 0, unroll=8)
+
+    def project(n, cc):
         def body():
             o = origin_of(n)
             left = gated[:, pl.ds(pl.multiple_of(o * shard_rows, LANES), shard_rows)]
             depth_rows = pl.ds(pl.multiple_of(o * shard_rows, 16), shard_rows)
 
             def one(j, carry):
-                cols = pl.ds(pl.multiple_of(j * shard_cols, LANES), shard_cols)
+                cols = pl.ds(pl.multiple_of((2 * j + cc) * shard_cols, LANES), shard_cols)
                 term = jnp.dot(
-                    left, held[lax.rem(j, 2), j // 2, depth_rows, :],
+                    left, held[cc, j, depth_rows, :],
                     preferred_element_type=jnp.float32,
                 )
                 if n == 0:
@@ -274,24 +283,12 @@
                     total[:, cols] += term
                 return carry
 
-            lax.fori_loop(0, 2 * chips, one, 0)
+            lax.fori_loop(0, chips, one, 0, unroll=4)
         when(n, body)
 
     per_block = BLOCK // CHUNK
     half = per_block // 2
 
-    events = [[lambda: turn(0)]]
-    for hop in range(1, depth):
-        up, down = 2 * hop - 1, 2 * hop
-        group = [functools.partial(recv_z, up), functools.partial(recv_z, down)]
-        events.append(group)
-        if hop == 1:
-            events.append([c_turn])
-        events.append([functools.partial(turn, up), functools.partial(turn, down)])
-        if hop == 1:
-            events.append([c_layer])
-        if hop > 1:
-            events.append([functools.partial(c_recv, up - 2), functools.partial(c_recv, down - 2)])
     work = [prepare]
     for b in range(block_count):
         def load(b=b):
@@ -299,27 +296,47 @@
             loads[b][1].wait()
             activate(b, 0, half)
         work += [load, functools.partial(activate, b, half, per_block), functools.partial(mix, b)]
-    while events or work:
-        for _ in range(2 if len(work) > 8 else 1):
-            if work:
-                work.pop(0)()
-        if events:
-            for event in events.pop(0):
-                event()
-
-    last = len(slots) - 2
-    finish(0)
-    finish(1)
-    finish(2)
-    recv_partner(0)
-    project(0)
-    for n in range(3, len(slots)):
-        finish(n)
-    c_recv(last)
-    c_recv(last + 1)
-    for n in range(1, len(slots)):
-        recv_partner(n)
-        project(n)
+
+    def do(count):
+        for step in work[:count]:
+            step()
+        del work[:count]
+
+    def each(event, hop):
+        for n in [0] if hop == 0 else [2 * hop - 1, 2 * hop]:
+            event(n)
+
+    def add(hop):
+        each(lambda n: project(n, core), hop)
+        each(recv_partner, hop)
+        each(lambda n: project(n, 1 - core), hop)
+
+    do(3)
+    c_turn()
+    turn(0)
+    do(2)
+    each(recv_z, 1)
+    do(1)
+    c_layer()
+    do(2)
+    for hop in range(2, depth):
+        each(recv_z, hop)
+        do(1)
+        each(turn, hop - 1)
+        do(1)
+        each(c_recv, hop - 1)
+        each(finish, hop - 2)
+        do(len(work))
+        if hop > 2:
+            add(hop - 3)
+    each(turn, depth - 1)
+    do(len(work))
+    for hop in range(max(0, depth - 3), depth):
+        if hop == depth - 1:
+            each(c_recv, hop)
+        if hop >= max(0, depth - 2):
+            each(finish, hop)
+        add(hop)
     out_ref[...] = total[...].astype(out_ref.dtype)
 
     for n in range(len(slots)):
@@ -329,7 +346,8 @@
             o = origin_of(n)
             for name, part in (("xa", "a"), ("yb", "b"), ("xb", "b"), ("ya", "a"), ("ya2", "a"), ("xb2", "b")):
                 copy(held_at(core, chip, o, part), (name, n), to_x).wait_send()
-            copy(held_at(core, slice(None), o, "ab"), ("p", n), partner).wait_send()
+            for k in range(4):
+                copy(held_at(core, chip, o, "ab"), ("p", k, n), partner).wait_send()
             if rows_c:
                 copy(held_at(core, slice(None), o, "c"), ("pc", n), partner).wait_send()
             for direction, cond, target in (("up", has_above, above), ("down", has_below, below)):
@@ -346,7 +364,7 @@
 
 
 def semaphores(depth):
-    return 10 * (2 * depth - 1) + 3
+    return 13 * (2 * depth - 1) + 3
 
 
 def fused(depth, columns, up_rows, mix_rows, ln_gain, mix_weight, mix_bias, out_weight):
@@ -359,11 +377,13 @@
     vmem = pl.BlockSpec(memory_space=pltpu.VMEM)
     return pl.pallas_call(
         functools.partial(kernel, depth, rows_c),
-        out_shape=jax.ShapeDtypeStruct((rows, shard_cols * columns), jnp.bfloat16),
-        in_specs=[any_space, any_space, vmem, any_space, vmem, any_space],
+        out_shape=pltpu.VMEM((rows, shard_cols * columns), jnp.bfloat16),
+        in_specs=[any_space] * 6,
         out_specs=vmem,
         scratch_shapes=[
             pltpu.VMEM((2, chips, depth * shard_rows, shard_cols), jnp.bfloat16),
+            pltpu.VMEM((1, channels), jnp.float32),
+            pltpu.VMEM((groups, BLOCK), jnp.float32),
             pltpu.VMEM((rows, channels), jnp.bfloat16),
             pltpu.VMEM((rows, channels), jnp.bfloat16),
             pltpu.VMEM((groups, BLOCK, BLOCK), jnp.bfloat16),
@@ -373,7 +393,7 @@
             pltpu.VMEM((BLOCK, channels), jnp.bfloat16),
             pltpu.VMEM((rows, channels), jnp.bfloat16),
             pltpu.VMEM((rows, shard_cols * columns), jnp.float32),
-            pltpu.SemaphoreType.DMA((2 + 2 * (rows // BLOCK),)),
+            pltpu.SemaphoreType.DMA((4 + 2 * (rows // BLOCK),)),
             pltpu.SemaphoreType.DMA((semaphores(depth),)),
             pltpu.SemaphoreType.DMA((semaphores(depth),)),
         ],

time: 56.4 us -> 42.7 us (0.76)
  Pallas kernels: 53.4 us -> 41.2 us
  local copies, waits for them, and re-layouts: 2.73 us -> 1.15 us
    pallas_call x1, Pallas kernels: 53.4 us -> 41.2 us  [fused(): pl.pallas_call(functools.partial(kernel, depth, rows_c), out_shape=pltpu....]
    unnamed x1, local copies, waits for them, and re-layouts: 2.73 us -> 1.15 us
where the time goes in v2:
time: 42.7 us; the launch traced here: 42.3 us
  Pallas kernels  41.2 us (96%)
  local copies, waits for them, and re-layouts  1.15 us (3%)
    pallas_call x1, Pallas kernels, fused(): pl.pallas_call(functools.partial(kernel, depth, rows_c), out_shape=pltpu....  41.2 us
    unnamed x1, local copies, waits for them, and re-layouts  1.15 us

profile of v2, /device:TPU:0, one launch (start us, length us, event | category | flops | bytes accessed | tf_op | source)
XLA Modules:
  0.0 42.3 jit_solution(9151820825130754715)
XLA Ops:
  0.0 41.2 %shard_map.64 = bf16[384,2048]{1,0:T(8,128)(2,1)S(1)} custom-call(bf16[384,2048]{1,0:T(8,128)(2,1)} %bitcast.5, bf16[384,2048]{1,0:T(8,128)(2,1)} %bitcast.6, f32[1,2048]{1,0:T(1,128)} %bitcast.7, bf16[16,128,128]{2,1,0:T(8,128)(2,1)} %weight_hbm.1, f32[16,128]{1,0:T(8,128)} %bias_hbm.1, bf16[512,256]{1,0:T(8,128)(2,1)} %shard_hbm.1), custom_call_target="tpu_custom_call" | custom-call | tf_op jit(solution)/shard_map/pallas_call | solution.py:378
  41.2 1.1 %copy.8 = bf16[1,384,2048]{2,1,0:T(8,128)(2,1)} copy(bf16[1,384,2048]{2,1,0:T(8,128)(2,1)S(1)} %bitcast.4) | data formatting | bytes 3145728
